TPU v7x, 256 devices: a 4x2x16 block of a 4x16x16 slice. The times are simulated.
256 devices in a mesh: grp: 2 (over y), fs: 32 (over z, core), tp: 4 (over x).
Axes of the slice: x: 4, y: 2, z: 16, core: 2. Of those that a mesh axis runs over, the one named last changes fastest.
The devices are a block of a 4x16x16 slice.
Arguments:
- prompt: bfloat16 [24576, 2048], P(('grp', 'fs')), parts along dimension 0, may hold values from -6 to 6
- routes: int32 [24576, 4], P(('grp', 'fs')), parts along dimension 0, may hold values from 0 to 31, all different within a row; in each aligned block of 384 rows (0 to 383, 384 to 767, ...) at most 60 rows name the same one
- route_weight: float32 [24576, 4], P(('grp', 'fs')), parts along dimension 0, may hold values from 0.2 to 1
- norm_gain: float32 [2048], P('fs'), may hold values from 0.1 to 1.9
- gate_train: float32 [32, 2048, 1024], P(None, 'fs', 'tp'), may hold values from -0.4 to 0.4
- up_train: float32 [32, 2048, 1024], P(None, 'fs', 'tp'), may hold values from -0.4 to 0.4
- down_train: float32 [32, 1024, 2048], P(None, 'fs', 'tp'), may hold values from -0.07 to 0.07
Outputs:
- gate_serve: bfloat16 [64, 2048, 1024], P(('grp', 'fs'), None, 'tp'), parts along dimension 0
- up_serve: bfloat16 [64, 2048, 1024], P(('grp', 'fs'), None, 'tp'), parts along dimension 0
- down_serve: bfloat16 [64, 1024, 2048], P(('grp', 'fs'), 'tp'), parts along dimension 0
- mixed: bfloat16 [24576, 2048], P(('grp', 'fs'), 'tp'), parts along dimension 0
There are 2 independent parts, one for each index of `grp`. A program takes and returns all parts, laid end to end along the dimension named above; an argument that names none is the same for every part. Nothing has to cross between parts.
Inputs may be any that keep to these rules, and one draw needn't show every extreme that they name: `routes`: each row names 4 different experts. Among the rows of one index of fs no expert is named more than 60 times, a bound that some block reaches on some index.
All inputs are finite; a program needn't handle non-finite values.
Results may differ from a plain program's by a relative error of at most 0.012.
Values may be sent and summed in bfloat16 or wider, within the bound.
A program may use at most 128 MiB of HBM per device.

v0:
```python
import jax
import jax.numpy as jnp
from jax import lax
from jax.sharding import Mesh
from jax.sharding import PartitionSpec as P

TOP = 4
FS = ("fs_0", "fs_1")
GRP_FS = ("grp", "fs_0", "fs_1")
LIMIT = 7.0
ALPHA = 1.702
EPS = 1e-06


def in_one_piece(arrays, axis, split_dim, concat_dim, along):
    both = jnp.concatenate(arrays, axis=along)
    out, at, outs = (
        lax.all_to_all(both, axis, split_axis=split_dim, concat_axis=concat_dim, tiled=True),
        0,
        [],
    )
    for a in arrays:
        outs.append(lax.slice_in_dim(out, at, at + a.shape[along], axis=along))
        at += a.shape[along]
    return tuple(outs)


def cut_along(value, dim, devices):
    before, after = (value.shape[:dim], value.shape[dim + 1 :])
    return jnp.moveaxis(value.reshape(*before, devices, -1, *after), dim, 0)


def joined_along(pieces, dim):
    pieces = jnp.moveaxis(pieces, 0, dim)
    dims = pieces.shape
    return pieces.reshape(*dims[:dim], dims[dim] * dims[dim + 1], *dims[dim + 2 :])


def moved_by_axis(pieces, axes, turns):
    inside = pieces.shape[1:]
    out = pieces.reshape(*(lax.axis_size(a) for a in axes), *inside)
    for k in turns:
        out = lax.all_to_all(out, axes[k], k, k, tiled=True)
    return out.reshape(-1, *inside)


def exchange_by_chip(value, groups, turns, split_dim, concat_dim):
    devices = lax.axis_size(groups[0]) * lax.axis_size(groups[1])
    pieces = cut_along(value, split_dim, devices)
    return joined_along(moved_by_axis(pieces, groups, turns), concat_dim)


def shards(prompt, routes, route_weight, norm_gain, gate_train, up_train, down_train):
    gate_cast = (norm_gain[None, :, None] * gate_train).astype(jnp.bfloat16)
    up_cast = (norm_gain[None, :, None] * up_train).astype(jnp.bfloat16)
    down_cast = down_train.astype(jnp.bfloat16)
    gate_mine, up_mine, down_rows = (
        *in_one_piece((gate_cast, up_cast), FS, 0, 1, 2),
        lax.all_to_all(down_cast, FS, split_axis=0, concat_axis=1, tiled=True),
    )
    down_mine = lax.all_to_all(down_rows, "tp", split_axis=1, concat_axis=2, tiled=True)
    tok_rows, width = prompt.shape
    experts = gate_train.shape[0]
    quarter = width // lax.axis_size("tp")
    capacity = min(tok_rows, max(2, 5 * tok_rows * TOP // (4 * experts)))
    values = prompt.astype(jnp.float32)
    normed = (values * lax.rsqrt(jnp.mean(values * values, axis=-1, keepdims=True) + EPS)).astype(
        jnp.bfloat16
    )
    flat_expert = routes.reshape(-1)
    onehot = (flat_expert[:, None] == jnp.arange(experts, dtype=jnp.int32)[None, :]).astype(
        jnp.int32
    )
    earlier = jnp.cumsum(onehot, axis=0) - onehot
    slot_pos = jnp.sum(earlier * onehot, axis=1)
    target = flat_expert * capacity + slot_pos
    source_row = jnp.arange(tok_rows * TOP, dtype=jnp.int32) // TOP
    col_start = lax.axis_index("tp") * quarter
    own_cols = lax.dynamic_slice_in_dim(normed, col_start, quarter, 1)
    outbox = (
        jnp.zeros((experts * capacity, quarter), jnp.bfloat16).at[target].set(own_cols[source_row])
    )
    inbox_part = lax.all_to_all(
        outbox.reshape(experts, capacity, quarter), FS, split_axis=0, concat_axis=1, tiled=True
    )
    inbox = lax.all_gather(inbox_part, "tp", axis=2, tiled=True)
    gate_pre = jnp.einsum("erd,edf->erf", inbox, gate_mine, preferred_element_type=jnp.float32)
    up_pre = jnp.einsum("erd,edf->erf", inbox, up_mine, preferred_element_type=jnp.float32)
    gate_pre = jnp.minimum(gate_pre, LIMIT)
    up_pre = jnp.clip(up_pre, -LIMIT, LIMIT)
    hidden = ((up_pre + 1.0) * gate_pre * jax.nn.sigmoid(ALPHA * gate_pre)).astype(jnp.bfloat16)
    own_width = hidden.shape[2]
    empty = jnp.zeros((hidden.shape[0], hidden.shape[1], down_rows.shape[2]), jnp.float32)
    total = empty
    piece = lax.all_gather(hidden, "tp", axis=2, tiled=True)
    for index in range(piece.shape[2] // own_width):
        cols = piece[:, :, index * own_width : (index + 1) * own_width]
        weight_rows = lax.dynamic_slice_in_dim(down_rows, index * own_width, own_width, 1)
        part = jnp.einsum(
            "erf,efd->erd", cols, weight_rows, preferred_element_type=jnp.float32
        ).astype(jnp.bfloat16)
        total = total + part.astype(jnp.float32)
    summed = total.astype(jnp.bfloat16)
    back = exchange_by_chip(summed, ("fs_0", "fs_1"), (1, 0), 1, 0)
    picked = back.reshape(experts * capacity, quarter)[target].astype(jnp.float32)
    weighted = picked.reshape(tok_rows, TOP, quarter) * route_weight[:, :, None]
    mixed = jnp.sum(weighted, axis=1).astype(jnp.bfloat16)
    return (gate_mine, up_mine, down_mine, mixed)


def solution(mesh):
    finer = Mesh(
        mesh.devices.reshape(mesh.shape["grp"], 16, 2, mesh.shape["tp"]),
        ("grp", "fs_0", "fs_1", "tp"),
    )
    placed = (
        P(GRP_FS, None),
        P(GRP_FS, None),
        P(GRP_FS, None),
        P(FS),
        P(None, FS, "tp"),
        P(None, FS, "tp"),
        P(None, FS, "tp"),
    )
    return jax.shard_map(
        shards,
        mesh=finer,
        in_specs=placed,
        out_specs=(
            P(GRP_FS, None, "tp"),
            P(GRP_FS, None, "tp"),
            P(GRP_FS, "tp", None),
            P(GRP_FS, "tp"),
        ),
        check_vma=False,
    )
```

profile of v0, /device:TPU:40, one launch (start us, length us, event | category | flops | bytes accessed | tf_op | source)
XLA Modules:
  0.0 537.3 jit_solution(2255770798606577626)
XLA Ops:
  7.3 1.9 convert_element_type.79
  9.2 0.4 multiply_reduce_fusion.1
  9.7 0.1 eq.29
  9.9 0.1 eq.25
  10.1 0.7 fusion.28
  10.8 15.9 %reduce-window.6 = s32[32,12,128]{2,1,0:T(8,128)S(1)} reduce-window(s32[32,12,128]{2,1,0:T(8,128)} %fusion.28, s32[]{:T(128)} %constant.22.clone.1), window={size=1x1x128 pad=0_0x0_0x127_0}, to_apply=%region_0.0 | reduce-window | flops 6242304 | bytes 393220 | tf_op jit(solution)/shard_map/reduce-window
  26.7 0.8 slice.38
  27.5 1.1 copy.42
  28.8 0.8 broadcast_add_fusion
  29.8 0.2 mul.75
  29.9 0.6 pad_clamp_fusion.1
  30.5 1.0 fusion.31
  31.7 15.8 %scatter_custom_fusion = bf16[1920,512]{1,0:T(8,128)(2,1)} fusion(s32[1536]{0:T(1024)S(1)} %fusion.32, bf16[384,512]{1,0:T(8,128)(2,1)S(1)} %fusion.27, s32[2048]{0:T(1024)} %pad_clamp_fusion.1, bf16[]{:T(256)} %constant.15.clone.1), kind=kCustom, calls=%fused_computation.23 | custom fusion | bytes 1966592 | tf_op jit(solution)/shard_map/scatter | solution.py:81
  47.5 2.5 reshape.188
  50.0 124.9 %all_to_all.64 = bf16[32,60,512]{2,1,0:T(8,128)(2,1)} all-to-all(bf16[32,60,512]{2,1,0:T(8,128)(2,1)S(1)} %reshape.188), channel_id=1, replica_groups=mesh['grp'=2,'fs_0'=16,'fs_1'=2,'tp'=4] {'fs_0','fs_1'}, dimensions={0} | all-to-all | bytes 3932160 | tf_op jit(solution)/shard_map/all_to_all | solution.py:83
  174.9 3.9 all_to_all.55
  179.0 2.2 multiply_convert_fusion.1
  181.2 0.2 pad_maximum_fusion
  181.4 116.5 %all_to_all.65 = bf16[32,64,512]{2,1,0:T(8,128)(2,1)S(1)} all-to-all(bf16[32,64,512]{2,1,0:T(8,128)(2,1)S(1)} %pad_maximum_fusion), channel_id=1, replica_groups=mesh['grp'=2,'fs_0'=16,'fs_1'=2,'tp'=4] {'fs_0','fs_1'}, dimensions={0} | all-to-all | bytes 4194304 | tf_op jit(solution)/shard_map/all_to_all | solution.py:18
  298.0 6.2 %fusion.7 = f32[1920,256]{1,0:T(8,128)S(1)} fusion(bf16[1,1920,2048]{2,1,0:T(8,128)(2,1)} %all-gather.4.cloned.1.call-done, bf16[1,2048,256]{2,1,0:T(8,128)(2,1)S(1)} %get-tuple-element.17), kind=kOutput, calls=%fused_computation.15 | convolution fusion | flops 2013757440 | bytes 10878976 | tf_op jit(solution)/shard_map/erd,edf->erf/dot_general | solution.py:87
  304.3 3.6 fusion.19
  308.0 0.2 convert_element_type.76
  308.1 59.6 %all_to_all.66 = bf16[32,32,512]{2,1,0:T(8,128)(2,1)S(1)} all-to-all(bf16[32,32,512]{2,1,0:T(8,128)(2,1)S(1)} %convert_element_type.76), channel_id=1, replica_groups=mesh['grp'=2,'fs_0'=16,'fs_1'=2,'tp'=4] {'fs_0','fs_1'}, dimensions={0} | all-to-all | bytes 2097152 | tf_op jit(solution)/shard_map/all_to_all | solution.py:59
  367.8 1.6 copy.53
  369.4 0.5 broadcast.145
  369.9 8.0 %reduce.4 = bf16[1024,512]{1,0:T(8,128)(2,1)} reduce(bf16[1024,1,512]{2,1,0:T(2,128)(2,1)S(1)} %bitcast.86, bf16[]{:T(256)} %broadcast.145), dimensions={1}, to_apply=%bitcast.77.reduce_sub_computation | reduce | bytes 2097154
  377.9 3.7 reshape.234
  381.7 2.0 convolution_convert_fusion.1
  383.7 1.9 convolution_convert_fusion.2
  385.6 0.7 convolution_convert_fusion
  386.3 2.4 add_convert_fusion
  388.6 2.6 reshape_transpose_reshape.3
  391.3 1.1 copy.44
  392.4 5.3 all_to_all.67
  397.7 4.6 all-to-all-start.2
  402.3 3.3 copy.45
  405.6 12.1 %all-to-all-done.2 = bf16[4,2,65536]{2,1,0:T(2,128)(2,1)S(1)} async-done(((bf16[4,2,65536]{2,1,0:T(2,128)(2,1)}), bf16[4,2,65536]{2,1,0:T(2,128)(2,1)S(1)}, u32[]{:S(2)}, u32[]{:S(2)}) %all-to-all-start.2) | async-done | bytes 1048608 | tf_op jit(solution)/shard_map/all_to_all | solution.py:61
  417.7 4.8 all-to-all-start.5
  422.7 1.0 reshape.235
  423.6 0.3 copy.49
  423.9 0.5 copy.38
  424.5 1.4 copy.48
  425.9 86.9 %all-to-all-done.5 = bf16[16,2,1,60,512]{4,1,3,2,0:T(2,128)(2,1)} async-done(((bf16[16,2,1,60,512]{4,1,3,2,0:T(2,128)(2,1)}), bf16[16,2,1,60,512]{4,1,3,2,0:T(2,128)(2,1)}, u32[]{:S(2)}, u32[]{:S(2)}) %all-to-all-start.5) | async-done | bytes 1966112 | tf_op jit(solution)/shard_map/all_to_all | solution.py:43
  512.8 3.3 copy.46
  516.1 2.5 reshape_reshape_reshape.3
  518.6 5.4 %gather_fusion = bf16[1536,512]{1,0:T(8,128)(2,1)} fusion(bf16[1920,512]{1,0:T(8,128)(2,1)S(1)} %reshape_reshape_reshape.3, s32[2048]{0:T(1024)S(1)} %pad_clamp_fusion), kind=kCustom, calls=%fused_computation.1 | custom fusion | bytes 3151872 | tf_op jit(solution)/shard_map/gather | solution.py:105
  524.1 2.8 reshape.200
  526.8 3.2 multiply_reduce_fusion
  (38 shorter events, 1.2 us)
Async XLA Ops:
  7.2 290.9 %all-gather.4.cloned.1.call-start = ((), (), s32[]{:S(2)}) async-start(), calls=%async_computation.6 | async-start | bytes 9830400 | tf_op jit(solution)/shard_map/all_gather | solution.py:86
  7.2 1.9 copy-start
  7.3 2.3 copy-start.6
  174.9 4.1 copy-start.2
  174.9 4.1 copy-start.8
  178.9 202.7 %all-gather.6.cloned.1.call-start = ((), (), s32[]{:S(2)}) async-start(), calls=%async_computation.7 | async-start | bytes 4915200 | tf_op jit(solution)/shard_map/all_gather | solution.py:95
  298.0 6.3 %copy-start.5 = (bf16[1,2048,256]{2,1,0:T(8,128)(2,1)}, bf16[1,2048,256]{2,1,0:T(8,128)(2,1)S(1)}, u32[]{:S(2)}) copy-start(bf16[1,2048,256]{2,1,0:T(8,128)(2,1)S(1)} %get-tuple-element.17) | copy-start | bytes 3145732
  298.0 6.3 %copy-start.4 = (bf16[1,2048,256]{2,1,0:T(8,128)(2,1)}, bf16[1,2048,256]{2,1,0:T(8,128)(2,1)S(1)}, u32[]{:S(2)}) copy-start(bf16[1,2048,256]{2,1,0:T(8,128)(2,1)S(1)} %get-tuple-element.16) | copy-start | bytes 3145732
  298.0 6.2 %copy-start.9 = (bf16[1,1920,2048]{2,1,0:T(8,128)(2,1)S(1)}, bf16[1,1920,2048]{2,1,0:T(8,128)(2,1)}, u32[]{:S(2)}) copy-start(bf16[1,1920,2048]{2,1,0:T(8,128)(2,1)} %all-gather.4.cloned.1.call-done) | copy-start | bytes 23592964
  304.3 3.7 copy-start.3
  381.7 3.9 copy-start.1
  397.7 20.0 %all-to-all-start.2 = ((bf16[4,2,65536]{2,1,0:T(2,128)(2,1)}), bf16[4,2,65536]{2,1,0:T(2,128)(2,1)S(1)}, u32[]{:S(2)}, u32[]{:S(2)}) async-start(bf16[4,2,65536]{2,1,0:T(2,128)(2,1)} %reshape.234), calls=%async_computation.2 | async-start | bytes 2097152 | tf_op jit(solution)/shard_map/all_to_all | solution.py:61
  405.6 16.9 %copy-start.7 = (f32[384,4]{0,1:T(4,128)S(1)}, f32[384,4]{0,1:T(4,128)}, u32[]{:S(2)}) copy-start(f32[384,4]{0,1:T(4,128)} %param.9) | copy-start | bytes 18436
  417.7 95.2 %all-to-all-start.5 = ((bf16[16,2,1,60,512]{4,1,3,2,0:T(2,128)(2,1)}), bf16[16,2,1,60,512]{4,1,3,2,0:T(2,128)(2,1)}, u32[]{:S(2)}, u32[]{:S(2)}) async-start(bf16[16,2,1,60,512]{4,1,3,2,0:T(2,128)(2,1)} %copy.45), calls=%async_computation.5 | async-start | bytes 3932160 | tf_op jit(solution)/shard_map/all_to_all | solution.py:43
Sparse Core Ops, SparseCore 0:
  179.0 76.8 all-gather.3
  308.1 46.6 all-gather.5
where the time goes:
time: 547 us; the launch traced here: 537 us
  blocking collectives  306 us (56%)
  waiting for transfers between devices  99.1 us (18%)
  local copies, waits for them, and re-layouts  55.4 us (10%)
  other arithmetic  35.3 us (6%)
  matrix products  16.7 us (3%)
  between operations  14.8 us (3%)
  starting transfers between devices  9.51 us (2%)
    all_to_all x1, blocking collectives, shards(): lax.all_to_all(outbox.reshape(experts, capacity, quarter), FS, split_axis...  125 us
    all_to_all x1, blocking collectives, in_one_piece(): lax.all_to_all(both, axis, split_axis=split_dim, concat_axis=concat_dim,...  116 us
    all_to_all x1, waiting for transfers between devices, moved_by_axis(): out = lax.all_to_all(out, axes[k], k, k, tiled=True)  86.9 us
    all_to_all x1, blocking collectives, shards(): lax.all_to_all(down_cast, FS, split_axis=0, concat_axis=1, tiled=True)  59.6 us
    another operation x3, other arithmetic  16.8 us
    scatter x1, local copies, waits for them, and re-layouts, shards(): jnp.zeros((experts * capacity, quarter), jnp.bfloat16).at[target]  15.8 us
    all_to_all x1, waiting for transfers between devices, shards(): lax.all_to_all(down_rows, 'tp', split_axis=1, concat_axis=2, tiled=True)  12.1 us
  transfers between devices with their start and end apart: 4, of which 2 were waited for; matrix products, arithmetic and copies ran while one was open for 4% of the time, Pallas kernels for 0%

commit v1 on v0

--- a/solution.py
+++ b/solution.py
@@ -56,7 +56,10 @@
     down_cast = down_train.astype(jnp.bfloat16)
     gate_mine, up_mine, down_rows = (
         *in_one_piece((gate_cast, up_cast), FS, 0, 1, 2),
-        lax.all_to_all(down_cast, FS, split_axis=0, concat_axis=1, tiled=True),
+        jnp.concatenate(
+            lax.all_to_all(jnp.stack(jnp.split(down_cast, lax.axis_size(FS), axis=0)), FS, 0, 0),
+            axis=1,
+        ),
     )
     down_mine = lax.all_to_all(down_rows, "tp", split_axis=1, concat_axis=2, tiled=True)
     tok_rows, width = prompt.shape

time: 547 us -> 545 us (level)
  blocking collectives: 306 us -> 191 us
  waiting for transfers between devices: 99.1 us -> 171 us
  local copies, waits for them, and re-layouts: 55.4 us -> 76.7 us
  starting transfers between devices: 9.51 us -> 26.7 us
    all_to_all x2 -> x1, blocking collectives: 176 us -> 60.5 us  [shards(): lax.all_to_all(jnp.stack(jnp.split(down_cast, lax.axis_size(FS), axis=0))...]
    all_to_all x0 -> x1, waiting for transfers between devices: none -> 72.3 us  [in_one_piece(): lax.all_to_all(both, axis, split_axis=split_dim, concat_axis=concat_dim,...]
    unnamed x27 -> x54, local copies, waits for them, and re-layouts: 7.25 us -> 26.6 us
    all_gather x1, starting transfers between devices: 0.07 us -> 12.3 us  [shards(): piece = lax.all_gather(hidden, 'tp', axis=2, tiled=True)]
  transfers between devices with their start and end apart: 4 -> 5, of which waited for: 2 -> 3; matrix products, arithmetic and copies ran while one was open for 4% -> 9% of each run, Pallas kernels for 0% -> 0%
where the time goes in v1:
time: 545 us; the launch traced here: 535 us
  blocking collectives  191 us (35%)
  waiting for transfers between devices  171 us (31%)
  local copies, waits for them, and re-layouts  76.7 us (14%)
  other arithmetic  38.4 us (7%)
  starting transfers between devices  26.7 us (5%)
  matrix products  16.3 us (3%)
  between operations  14.8 us (3%)
    all_to_all x1, blocking collectives, shards(): lax.all_to_all(outbox.reshape(experts, capacity, quarter), FS, split_axis...  125 us
    all_to_all x1, waiting for transfers between devices, moved_by_axis(): out = lax.all_to_all(out, axes[k], k, k, tiled=True)  86.9 us
    all_to_all x1, waiting for transfers between devices, in_one_piece(): lax.all_to_all(both, axis, split_axis=split_dim, concat_axis=concat_dim,...  72.3 us
    all_to_all x1, blocking collectives, shards(): lax.all_to_all(jnp.stack(jnp.split(down_cast, lax.axis_size(FS), axis=0))...  60.5 us
    unnamed x54, local copies, waits for them, and re-layouts  26.6 us
    another operation x3, other arithmetic  16.8 us
    scatter x1, local copies, waits for them, and re-layouts, shards(): jnp.zeros((experts * capacity, quarter), jnp.bfloat16).at[target]  15.8 us
    all_gather x1, starting transfers between devices, shards(): piece = lax.all_gather(hidden, 'tp', axis=2, tiled=True)  12.3 us
  transfers between devices with their start and end apart: 5, of which 3 were waited for; matrix products, arithmetic and copies ran while one was open for 9% of the time, Pallas kernels for 0%

profile of v1, /device:TPU:40, one launch (start us, length us, event | category | flops | bytes accessed | tf_op | source)
XLA Modules:
  0.0 535.1 jit_solution(4909778127345454928)
XLA Ops:
  7.3 1.9 convert_element_type.79
  10.1 0.7 fusion.28
  10.8 15.9 %reduce-window.6 = s32[32,12,128]{2,1,0:T(8,128)S(1)} reduce-window(s32[32,12,128]{2,1,0:T(8,128)} %fusion.28, s32[]{:T(128)} %constant.22.clone.1), window={size=1x1x128 pad=0_0x0_0x127_0}, to_apply=%region_0.0 | reduce-window | flops 6242304 | bytes 393220 | tf_op jit(solution)/shard_map/reduce-window
  26.7 0.8 slice.38
  27.5 1.1 copy.85
  28.8 0.8 broadcast_add_fusion
  30.5 1.0 fusion.31
  31.7 15.8 %scatter_custom_fusion = bf16[1920,512]{1,0:T(8,128)(2,1)} fusion(s32[1536]{0:T(1024)S(1)} %fusion.32, bf16[384,512]{1,0:T(8,128)(2,1)S(1)} %fusion.27, s32[2048]{0:T(1024)} %pad_clamp_fusion.1, bf16[]{:T(256)} %constant.15.clone.1), kind=kCustom, calls=%fused_computation.23 | custom fusion | bytes 1966592 | tf_op jit(solution)/shard_map/scatter | solution.py:84
  47.5 2.5 reshape.189
  50.0 124.9 %all_to_all.57 = bf16[32,60,512]{2,1,0:T(8,128)(2,1)} all-to-all(bf16[32,60,512]{2,1,0:T(8,128)(2,1)S(1)} %reshape.189), channel_id=1, replica_groups=mesh['grp'=2,'fs_0'=16,'fs_1'=2,'tp'=4] {'fs_0','fs_1'}, dimensions={0} | all-to-all | bytes 3932160 | tf_op jit(solution)/shard_map/all_to_all | solution.py:86
  174.9 3.9 all_to_all.48
  178.9 2.2 multiply_convert_fusion.1
  181.1 1.6 pad_maximum_fusion
  182.7 4.9 all-to-all-start
  187.6 12.3 %all-gather.6.cloned.1.call-start = ((), (), s32[]{:S(2)}) async-start(), calls=%async_computation.7 | async-start | bytes 4915200 | tf_op jit(solution)/shard_map/all_gather | solution.py:98
  199.9 1.8 convert_element_type.76
  201.7 0.6 constant_dynamic-update-slice_fusion.31
  209.1 0.6 constant_dynamic-update-slice_fusion.19
  213.5 0.6 constant_dynamic-update-slice_fusion.12
  215.9 72.3 %all-to-all-done = bf16[32,64,512]{2,1,0:T(8,128)(2,1)S(1)} async-done(((bf16[32,64,512]{2,1,0:T(8,128)(2,1)}), bf16[32,64,512]{2,1,0:T(8,128)(2,1)S(1)}, u32[]{:S(2)}, u32[]{:S(2)}) %all-to-all-start) | async-done | bytes 2097184 | tf_op jit(solution)/shard_map/all_to_all | solution.py:18
  288.3 1.5 fusion.34
  289.7 5.8 %fusion.7 = f32[1920,256]{1,0:T(8,128)S(1)} fusion(bf16[1,1920,2048]{2,1,0:T(8,128)(2,1)} %all-gather.4.cloned.1.call-done, bf16[1,2048,256]{2,1,0:T(8,128)(2,1)} %get-tuple-element.21), kind=kOutput, calls=%fused_computation.15 | convolution fusion | flops 2013757440 | bytes 10878976 | tf_op jit(solution)/shard_map/erd,edf->erf/dot_general | solution.py:90
  295.8 3.6 fusion.19
  299.5 0.6 constant_dynamic-update-slice_fusion.8
  303.2 0.6 constant_dynamic-update-slice_fusion.2
  305.0 60.5 %all_to_all.58 = bf16[32,1,32,512]{3,2,1,0:T(8,128)(2,1)S(1)} all-to-all(bf16[32,1,32,512]{3,2,1,0:T(8,128)(2,1)} %constant_dynamic-update-slice_fusion), channel_id=1, replica_groups=mesh['grp'=2,'fs_0'=16,'fs_1'=2,'tp'=4] {'fs_0','fs_1'}, dimensions={0} | all-to-all | bytes 2097152 | tf_op jit(solution)/shard_map/all_to_all | solution.py:60
  365.6 1.6 copy.96
  367.7 8.0 %reduce.4 = bf16[1024,512]{1,0:T(8,128)(2,1)} reduce(bf16[1024,1,512]{2,1,0:T(2,128)(2,1)S(1)} %bitcast.214, bf16[]{:T(256)} %broadcast.145), dimensions={1}, to_apply=%bitcast.205.reduce_sub_computation | reduce | bytes 2097154
  375.7 3.7 reshape.235
  379.5 2.0 convolution_convert_fusion.2
  381.5 1.9 convolution_convert_fusion.1
  383.4 0.7 convolution_convert_fusion
  384.1 2.4 add_convert_fusion
  386.4 2.6 reshape_transpose_reshape.3
  389.1 1.1 copy.87
  390.2 5.3 all_to_all.59
  395.5 4.6 all-to-all-start.2
  400.1 3.3 copy.88
  403.4 12.1 %all-to-all-done.2 = bf16[4,2,65536]{2,1,0:T(2,128)(2,1)S(1)} async-done(((bf16[4,2,65536]{2,1,0:T(2,128)(2,1)}), bf16[4,2,65536]{2,1,0:T(2,128)(2,1)S(1)}, u32[]{:S(2)}, u32[]{:S(2)}) %all-to-all-start.2) | async-done | bytes 1048608 | tf_op jit(solution)/shard_map/all_to_all | solution.py:64
  415.5 4.8 all-to-all-start.5
  420.5 1.0 reshape.236
  422.3 1.4 copy.91
  423.7 86.9 %all-to-all-done.5 = bf16[16,2,1,60,512]{4,1,3,2,0:T(2,128)(2,1)} async-done(((bf16[16,2,1,60,512]{4,1,3,2,0:T(2,128)(2,1)}), bf16[16,2,1,60,512]{4,1,3,2,0:T(2,128)(2,1)}, u32[]{:S(2)}, u32[]{:S(2)}) %all-to-all-start.5) | async-done | bytes 1966112 | tf_op jit(solution)/shard_map/all_to_all | solution.py:43
  510.6 3.3 copy.89
  514.0 2.5 reshape_reshape_reshape.3
  516.5 5.4 %gather_fusion = bf16[1536,512]{1,0:T(8,128)(2,1)} fusion(bf16[1920,512]{1,0:T(8,128)(2,1)S(1)} %reshape_reshape_reshape.3, s32[2048]{0:T(1024)S(1)} %pad_clamp_fusion), kind=kCustom, calls=%fused_computation.1 | custom fusion | bytes 3151872 | tf_op jit(solution)/shard_map/gather | solution.py:108
  521.9 2.8 reshape.201
  524.7 3.2 multiply_reduce_fusion
  (67 shorter events, 20.6 us)
Async XLA Ops:
  7.2 282.5 %all-gather.4.cloned.1.call-start = ((), (), s32[]{:S(2)}) async-start(), calls=%async_computation.6 | async-start | bytes 9830400 | tf_op jit(solution)/shard_map/all_gather | solution.py:89
  7.2 1.9 copy-start
  7.3 2.3 copy-start.4
  174.9 4.0 copy-start.2
  174.9 4.0 copy-start.6
  182.7 105.6 %all-to-all-start = ((bf16[32,64,512]{2,1,0:T(8,128)(2,1)}), bf16[32,64,512]{2,1,0:T(8,128)(2,1)S(1)}, u32[]{:S(2)}, u32[]{:S(2)}) async-start(bf16[32,64,512]{2,1,0:T(8,128)(2,1)} %pad_maximum_fusion), calls=%async_computation | async-start | bytes 4194304 | tf_op jit(solution)/shard_map/all_to_all | solution.py:18
  187.6 191.9 %all-gather.6.cloned.1.call-start = ((), (), s32[]{:S(2)}) async-start(), calls=%async_computation.7 | async-start | bytes 4915200 | tf_op jit(solution)/shard_map/all_gather | solution.py:98
  289.7 5.8 %copy-start.3 = (bf16[1,2048,256]{2,1,0:T(8,128)(2,1)S(1)}, bf16[1,2048,256]{2,1,0:T(8,128)(2,1)}, u32[]{:S(2)}) copy-start(bf16[1,2048,256]{2,1,0:T(8,128)(2,1)} %get-tuple-element.20) | copy-start | bytes 3145732
  289.7 6.1 %copy-start.7 = (bf16[1,1920,2048]{2,1,0:T(8,128)(2,1)S(1)}, bf16[1,1920,2048]{2,1,0:T(8,128)(2,1)}, u32[]{:S(2)}) copy-start(bf16[1,1920,2048]{2,1,0:T(8,128)(2,1)} %all-gather.4.cloned.1.call-done) | copy-start | bytes 23592964
  379.5 3.9 copy-start.1
  395.5 20.0 %all-to-all-start.2 = ((bf16[4,2,65536]{2,1,0:T(2,128)(2,1)}), bf16[4,2,65536]{2,1,0:T(2,128)(2,1)S(1)}, u32[]{:S(2)}, u32[]{:S(2)}) async-start(bf16[4,2,65536]{2,1,0:T(2,128)(2,1)} %reshape.235), calls=%async_computation.2 | async-start | bytes 2097152 | tf_op jit(solution)/shard_map/all_to_all | solution.py:64
  403.4 16.9 %copy-start.5 = (f32[384,4]{0,1:T(4,128)S(1)}, f32[384,4]{0,1:T(4,128)}, u32[]{:S(2)}) copy-start(f32[384,4]{0,1:T(4,128)} %param.9) | copy-start | bytes 18436
  415.5 95.2 %all-to-all-start.5 = ((bf16[16,2,1,60,512]{4,1,3,2,0:T(2,128)(2,1)}), bf16[16,2,1,60,512]{4,1,3,2,0:T(2,128)(2,1)}, u32[]{:S(2)}, u32[]{:S(2)}) async-start(bf16[16,2,1,60,512]{4,1,3,2,0:T(2,128)(2,1)} %copy.88), calls=%async_computation.5 | async-start | bytes 3932160 | tf_op jit(solution)/shard_map/all_to_all | solution.py:43
Sparse Core Ops, SparseCore 0:
  179.0 76.8 all-gather.3
  299.6 46.9 all-gather.5
